TPU v7x, 32 devices: a whole 2x2x4 slice. The times are simulated.
32 devices in a mesh: ep: 16 (over z, y, x), tp: 2 (over core).
Axes of the slice: x: 2, y: 2, z: 4, core: 2. Of those that a mesh axis runs over, the one named last changes fastest.
Arguments:
- tokens: bfloat16 [16, 2048], P('ep'), may hold values from -6 to 6
- norm_gain: float32 [2048], replicated, may hold values from 0.1 to 1.9
- w_query: bfloat16 [2048, 512], P('ep', 'tp'), may hold values from -0.125 to 0.125
- w_key: bfloat16 [2048, 512], P('ep', 'tp'), may hold values from -0.125 to 0.125
- w_value: bfloat16 [2048, 1024], P('ep', 'tp'), may hold values from -0.125 to 0.125
- w_outgate: bfloat16 [2048, 1024], P('ep', 'tp'), may hold values from -0.125 to 0.125
- decay_in: bfloat16 [2048, 16], replicated, may hold values from -0.125 to 0.125
- decay_out: bfloat16 [16, 512], P(None, 'tp'), may hold values from -1.5 to 1.5
- decay_bias: float32 [512], P('tp'), may hold values from -40 to 4
- gla_state: float32 [16, 2, 256, 512], P('ep', 'tp'), may hold values from -6 to 6
- head_gain: float32 [512], replicated, may hold values from 0.1 to 1.9
- w_output: bfloat16 [1024, 2048], P(None, 'ep'), may hold values from -0.1875 to 0.1875
- moe_gain: float32 [2048], replicated, may hold values from 0.1 to 1.9
- expert_ids: int32 [16, 6], replicated, may hold values from 0 to 15, all different within a row; in each aligned block of 16 rows (0 to 15, 16 to 31, ...) at most 12 rows name the same one
- route_weight: float32 [16, 6], replicated, may hold values from 0.2 to 1
- expert_gate: bfloat16 [16, 2048, 512], P('ep', None, 'tp'), may hold values from -0.125 to 0.125
- expert_up: bfloat16 [16, 2048, 512], P('ep', None, 'tp'), may hold values from -0.125 to 0.125
- expert_down: bfloat16 [16, 512, 2048], P('ep', 'tp'), may hold values from -0.25 to 0.25
- shared_gate: bfloat16 [2048, 512], P(None, 'tp'), may hold values from -0.125 to 0.125
- shared_up: bfloat16 [2048, 512], P(None, 'tp'), may hold values from -0.125 to 0.125
- shared_down: bfloat16 [512, 2048], P('tp'), may hold values from -0.25 to 0.25
Outputs:
- result: bfloat16 [16, 2048], P(None, 'ep')
- new_state: float32 [16, 2, 256, 512], P('ep', 'tp')
Inputs may be any that keep to these rules, and one draw needn't show every extreme that they name: `expert_ids`: each row names 6 different experts. No expert is named by more than 12 rows in all, a bound that some block reaches.
All inputs are finite; a program needn't handle non-finite values.
Results may differ from a plain program's by a relative error of at most 0.018.
Values may be sent and summed in bfloat16 or wider, within the bound.
No kernel may reach another device: no remote copies, remote signals or barrier semaphores. Data moves between devices by JAX's collectives and lax.ppermute only.
A program may use at most 64 MiB of HBM per device.

v0:
```python
import jax
import jax.numpy as jnp
from jax import lax
from jax.sharding import PartitionSpec as P

DK = 256
DV = 512


EPSILON = 1e-06
DECAY_TEMPER = 16.0


def rms_scale(values):
    return lax.rsqrt(jnp.mean(values * values, axis=-1, keepdims=True) + EPSILON)


def slot_positions(expert_ids, expert_count):
    flat_ids = expert_ids.reshape(-1)
    onehot = (flat_ids[:, None] == jnp.arange(expert_count, dtype=jnp.int32)[None, :]).astype(
        jnp.int32
    )
    before = jnp.cumsum(onehot, axis=0) - onehot
    position = jnp.sum(before * onehot, axis=1)
    return (flat_ids, position)


def expert_block(rows, moe_gain, gate_weight, up_weight, down_weight):
    row_float = rows.astype(jnp.float32)
    normal_rows = (row_float * rms_scale(row_float) * moe_gain).astype(jnp.bfloat16)
    gate_values = jnp.einsum(
        "ecd,edf->ecf", normal_rows, gate_weight, preferred_element_type=jnp.float32
    )
    upward = jnp.einsum("ecd,edf->ecf", normal_rows, up_weight, preferred_element_type=jnp.float32)
    active = (jax.nn.silu(gate_values) * upward).astype(jnp.bfloat16)
    return jnp.einsum(
        "ecf,efd->ecd", active, down_weight, preferred_element_type=jnp.float32
    ).astype(jnp.bfloat16)


def per_device(
    tokens,
    norm_gain,
    w_query,
    w_key,
    w_value,
    w_outgate,
    decay_in,
    decay_out,
    decay_bias,
    gla_state,
    head_gain,
    w_output,
    moe_gain,
    expert_ids,
    route_weight,
    expert_gate,
    expert_up,
    expert_down,
    shared_gate,
    shared_up,
    shared_down,
):
    ep_size = lax.axis_size("ep")
    tp_size = lax.axis_size("tp")
    seq_dev = tokens.shape[0]
    top_count = expert_ids.shape[1]
    exp_dev = expert_gate.shape[0]
    experts = exp_dev * ep_size
    all_rows = seq_dev * ep_size
    capacity = 2 * seq_dev * top_count // exp_dev
    heads_local = w_query.shape[1] // DK
    tok_float = tokens.astype(jnp.float32)
    normed = (tok_float * rms_scale(tok_float) * norm_gain).astype(jnp.bfloat16)
    span_sizes = (w_query.shape[1], w_key.shape[1], w_value.shape[1], w_outgate.shape[1])
    raw_columns, normed_columns = (
        lax.all_to_all(tokens, "ep", split_axis=1, concat_axis=0, tiled=True),
        lax.all_to_all(normed, "ep", split_axis=1, concat_axis=0, tiled=True),
    )
    joined = lax.psum_scatter(
        jnp.concatenate(
            [
                jnp.dot(normed_columns, weight, preferred_element_type=jnp.float32)
                for weight in (w_query, w_key, w_value, w_outgate)
            ],
            axis=1,
        ),
        "ep",
        scatter_dimension=0,
        tiled=True,
    )
    column_edges = [
        0,
        span_sizes[0],
        span_sizes[0] + span_sizes[1],
        span_sizes[0] + span_sizes[1] + span_sizes[2],
        sum(span_sizes),
    ]
    projected = tuple(
        (joined[:, column_edges[number] : column_edges[number + 1]] for number in range(4))
    )
    query_rows, key_rows, value_rows, gate_rows = (
        part_sum.astype(jnp.bfloat16) for part_sum in projected
    )
    decay_low = jnp.dot(normed, decay_in, preferred_element_type=jnp.float32).astype(jnp.bfloat16)
    decay_pre = jnp.dot(decay_low, decay_out, preferred_element_type=jnp.float32) + decay_bias
    decay_rate = jnp.exp(jax.nn.log_sigmoid(decay_pre) / DECAY_TEMPER).reshape(
        seq_dev, heads_local, DK
    )
    query_heads = query_rows.astype(jnp.float32).reshape(seq_dev, heads_local, DK) * DK ** (-0.5)
    key_heads = key_rows.astype(jnp.float32).reshape(seq_dev, heads_local, DK)
    value_heads = value_rows.astype(jnp.float32).reshape(seq_dev, heads_local, DV)
    new_state = (
        decay_rate[..., None] * gla_state + key_heads[..., None] * value_heads[:, :, None, :]
    )
    read_out = jnp.einsum("shk,shkv->shv", query_heads, new_state, precision=lax.Precision.HIGHEST)
    gate_heads = gate_rows.astype(jnp.float32).reshape(seq_dev, heads_local, DV)
    mixed_heads = (read_out * rms_scale(read_out) * head_gain * jax.nn.silu(gate_heads)).astype(
        jnp.bfloat16
    )
    head_weights = w_output.reshape(tp_size, heads_local * DV, w_output.shape[1])
    shard_rows = lax.all_gather(mixed_heads, ("ep", "tp"), axis=0, tiled=True)
    owners = lax.iota(jnp.int32, shard_rows.shape[0])
    select = (owners[:, None] % tp_size == lax.iota(jnp.int32, tp_size)[None, :]).astype(
        jnp.bfloat16
    )
    chosen = jnp.einsum(
        "mt,tcd->mcd", select, head_weights, preferred_element_type=jnp.float32
    ).astype(jnp.bfloat16)
    spread = jnp.einsum("msc,mcd->msd", shard_rows, chosen, preferred_element_type=jnp.float32)
    attention = (
        spread.reshape(ep_size, tp_size, seq_dev, -1)
        .sum(axis=1)
        .reshape(all_rows, -1)
        .astype(jnp.bfloat16)
    )
    hidden = (raw_columns.astype(jnp.float32) + attention.astype(jnp.float32)).astype(jnp.bfloat16)
    flat_ids, position = slot_positions(expert_ids, experts)
    owner_rows = lax.iota(jnp.int32, all_rows * top_count) // top_count
    slot_table = (
        jnp.full((experts, capacity), all_rows, jnp.int32).at[flat_ids, position].set(owner_rows)
    )
    padded = jnp.concatenate([hidden, jnp.zeros((1, hidden.shape[1]), jnp.bfloat16)], axis=0)
    routed_rows, shared_rows = (
        lax.all_to_all(padded[slot_table], "ep", split_axis=0, concat_axis=2, tiled=True),
        lax.all_to_all(
            hidden.reshape(ep_size, seq_dev, hidden.shape[1]),
            "ep",
            split_axis=0,
            concat_axis=2,
            tiled=True,
        ),
    )
    routed_part = expert_block(routed_rows, moe_gain, expert_gate, expert_up, expert_down)
    shared_part = expert_block(
        shared_rows, moe_gain, shared_gate[None], shared_up[None], shared_down[None]
    )
    routed_sum, shared_sum = (
        lax.psum(routed_part, "tp").astype(jnp.float32),
        lax.psum(shared_part, "tp").astype(jnp.float32),
    )
    routed_out = routed_sum.astype(jnp.bfloat16)
    shared_out = shared_sum.astype(jnp.bfloat16)
    back_routed, back_shared = (
        lax.all_to_all(routed_out, "ep", split_axis=2, concat_axis=0, tiled=True),
        lax.all_to_all(shared_out, "ep", split_axis=2, concat_axis=0, tiled=True),
    )
    picked = back_routed.reshape(experts * capacity, -1)[flat_ids * capacity + position]
    weighted = picked.astype(jnp.float32).reshape(all_rows, top_count, -1) * route_weight[..., None]
    moe_columns = jnp.sum(weighted, axis=1) + back_shared.reshape(all_rows, -1).astype(jnp.float32)
    result = (hidden.astype(jnp.float32) + moe_columns).astype(jnp.bfloat16)
    return (result, new_state)


def solution(mesh):
    return jax.shard_map(
        per_device,
        mesh=mesh,
        in_specs=(
            P("ep", None),
            P(),
            P("ep", "tp"),
            P("ep", "tp"),
            P("ep", "tp"),
            P("ep", "tp"),
            P(),
            P(None, "tp"),
            P("tp"),
            P("ep", "tp", None, None),
            P(),
            P(None, "ep"),
            P(),
            P(),
            P(),
            P("ep", None, "tp"),
            P("ep", None, "tp"),
            P("ep", "tp", None),
            P(None, "tp"),
            P(None, "tp"),
            P("tp", None),
        ),
        out_specs=(P(None, "ep"), P("ep", "tp", None, None)),
        check_vma=False,
    )
```

profile of v0, /device:TPU:0, one launch (start us, length us, event | category | flops | bytes accessed | tf_op | source)
XLA Modules:
  0.0 244.8 jit_solution(1949194534503189319)
XLA Ops:
  0.7 1.4 multiply_reduce_fusion.2
  4.1 8.3 %all-to-all-start.1 = ((bf16[1,16,128]{2,0,1:T(2,128)(2,1)}), bf16[1,16,128]{2,0,1:T(2,128)(2,1)S(1)}, u32[]{:S(2)}, u32[]{:S(2)}) async-start(bf16[1,16,128]{2,0,1:T(2,128)(2,1)} %convert_bitcast_fusion.3), calls=%async_computation.1 | async-start | bytes 16384 | tf_op jit(solution)/shard_map/all_to_all | solution.py:78
  13.9 5.4 %scatter_fusion = s32[16,12]{1,0:T(8,128)S(1)} fusion(s32[16,12]{1,0:T(8,128)S(1)} %broadcast_in_dim.7, s32[96]{0:T(128)S(1)} %get-tuple-element.7, s32[96]{0:T(128)S(1)} %and_select_fusion), kind=kCustom, calls=%fused_computation.2 | custom fusion | bytes 1920 | tf_op jit(solution)/shard_map/scatter | solution.py:141
  21.2 4.2 %convolution_convert_fusion = bf16[32,512,128]{2,0,1:T(8,128)(2,1)} fusion(bf16[2,512,128]{2,1,0:T(8,128)(2,1)} %bitcast.143, s32[32]{0:T(128)S(1)} %and_select_fusion.1), kind=kOutput, calls=%fused_computation.5 | convolution fusion | flops 10485824 | bytes 4456576 | tf_op jit(solution)/shard_map/mt,tcd->mcd/dot_general | solution.py:127
  26.1 6.9 %all-to-all-start = ((bf16[1,16,128]{2,0,1:T(2,128)(2,1)}), bf16[1,16,128]{2,0,1:T(2,128)(2,1)S(1)}, u32[]{:S(2)}, u32[]{:S(2)}) async-start(bf16[1,16,128]{2,0,1:T(2,128)(2,1)} %bitcast), calls=%async_computation | async-start | bytes 16384 | tf_op jit(solution)/shard_map/all_to_all | solution.py:77
  33.5 78.2 %all-reduce.1 = bf16[16,1536]{1,0:T(8,128)(2,1)S(1)} all-reduce(f32[16,1536]{1,0:T(8,128)S(1)} %pad_maximum_fusion), channel_id=3, replica_groups=mesh['ep'=16,'tp'=2] {'ep'}, use_global_device_ids=true, to_apply=%region_1.0.clone | all-reduce | flops 24576 | bytes 147456
  116.1 36.5 %all-gather.1 = bf16[32,1,512]{2,1,0:T(2,128)(2,1)S(1)} all-gather(bf16[1,1,512]{2,1,0:T(2,128)(2,1)S(1)} %reshape.496), channel_id=2, replica_groups=mesh['ep'=16,'tp'=2] {'ep','tp'}, dimensions={0}, use_global_device_ids=true | all-gather | bytes 33792 | tf_op jit(solution)/shard_map/all_gather | solution.py:122
  152.6 6.4 %fusion = f32[32,1,128]{2,1,0:T(1,128)S(1)} fusion(bf16[32,512,128]{2,0,1:T(8,128)(2,1)} %convolution_convert_fusion, bf16[32,1,512]{2,1,0:T(2,128)(2,1)S(1)} %all-gather.1), kind=kOutput, calls=%fused_computation.3 | convolution fusion | flops 4194304 | bytes 4243456 | tf_op jit(solution)/shard_map/msc,mcd->msd/dot_general | solution.py:130
  159.7 3.4 %all-to-all-start.4 = ((bf16[16,1,128]{2,1,0:T(2,128)(2,1)}), bf16[16,1,128]{2,1,0:T(2,128)(2,1)S(1)}, u32[]{:S(2)}, u32[]{:S(2)}) async-start(bf16[16,1,128]{2,1,0:T(2,128)(2,1)} %copy.73), calls=%async_computation.4 | async-start | bytes 16384 | tf_op jit(solution)/shard_map/all_to_all | solution.py:146
  164.6 5.8 %all-to-all-done.4 = bf16[16,1,128]{2,1,0:T(2,128)(2,1)S(1)} async-done(((bf16[16,1,128]{2,1,0:T(2,128)(2,1)}), bf16[16,1,128]{2,1,0:T(2,128)(2,1)S(1)}, u32[]{:S(2)}, u32[]{:S(2)}) %all-to-all-start.4) | async-done | bytes 4128 | tf_op jit(solution)/shard_map/all_to_all | solution.py:146
  170.4 3.5 %all-to-all-start.2 = ((bf16[16,12,128]{2,1,0:T(8,128)(2,1)}), bf16[16,12,128]{2,1,0:T(8,128)(2,1)S(1)}, u32[]{:S(2)}, u32[]{:S(2)}) async-start(bf16[16,12,128]{2,1,0:T(8,128)(2,1)} %reshape.471), calls=%async_computation.2 | async-start | bytes 131072 | tf_op jit(solution)/shard_map/all_to_all | solution.py:145
  175.8 1.5 fusion.66
  177.3 4.1 %all-to-all-done.2 = bf16[16,12,128]{2,1,0:T(8,128)(2,1)S(1)} async-done(((bf16[16,12,128]{2,1,0:T(8,128)(2,1)}), bf16[16,12,128]{2,1,0:T(8,128)(2,1)S(1)}, u32[]{:S(2)}, u32[]{:S(2)}) %all-to-all-start.2) | async-done | bytes 49184 | tf_op jit(solution)/shard_map/all_to_all | solution.py:145
  181.7 1.5 fusion.9
  183.2 2.0 fusion.2
  185.1 3.6 %all-reduce.2 = (bf16[1,12,2048]{2,1,0:T(8,128)(2,1)S(1)}, bf16[1,1,2048]{2,1,0:T(2,128)(2,1)S(1)}) all-reduce(bf16[1,12,2048]{2,1,0:T(8,128)(2,1)S(1)} %fusion.2, bf16[1,1,2048]{2,1,0:T(2,128)(2,1)S(1)} %convert_element_type.218), channel_id=1, replica_groups=mesh['ep'=16,'tp'=2] {'tp'}, use_global_device_ids=true, to_apply=%region_8.9 | all-reduce | flops 26624 | bytes 106496 | tf_op jit(solution)/shard_map/psum | solution.py:159
  188.7 2.1 copy.74
  190.8 3.8 %all-to-all-start.5 = ((bf16[1,1,2048]{1,0,2:T(2,128)(2,1)}), bf16[1,1,2048]{1,0,2:T(2,128)(2,1)S(1)}, u32[]{:S(2)}, u32[]{:S(2)}) async-start(bf16[1,1,2048]{1,0,2:T(2,128)(2,1)} %copy.74), calls=%async_computation.5 | async-start | bytes 2097152 | tf_op jit(solution)/shard_map/all_to_all | solution.py:166
  196.1 12.4 %reduce.11 = bf16[2048,12]{1,0:T(8,128)(2,1)} reduce(bf16[2048,1,12]{2,1,0:T(2,128)(2,1)S(1)} %bitcast.139, bf16[]{:T(256)} %broadcast.257), dimensions={1}, to_apply=%bitcast.122.reduce_sub_computation | reduce | bytes 98306
  208.4 2.4 reshape.519
  210.9 8.5 %all-to-all-done.5 = bf16[1,1,2048]{1,0,2:T(2,128)(2,1)S(1)} async-done(((bf16[1,1,2048]{1,0,2:T(2,128)(2,1)}), bf16[1,1,2048]{1,0,2:T(2,128)(2,1)S(1)}, u32[]{:S(2)}, u32[]{:S(2)}) %all-to-all-start.5) | async-done | bytes 4128 | tf_op jit(solution)/shard_map/all_to_all | solution.py:166
  219.3 6.8 %all-to-all-start.3 = ((bf16[16,2,768]{2,1,0:T(2,128)(2,1)}), bf16[16,2,768]{2,1,0:T(2,128)(2,1)S(1)}, u32[]{:S(2)}, u32[]{:S(2)}) async-start(bf16[16,2,768]{2,1,0:T(2,128)(2,1)} %reshape.519), calls=%async_computation.3 | async-start | bytes 98304 | tf_op jit(solution)/shard_map/all_to_all | solution.py:165
  226.1 15.2 %convert_reduce_fusion = f32[2048]{0:T(1024)S(1)} fusion(bf16[1,1,2048]{1,0,2:T(2,128)(2,1)S(1)} %all-to-all-done.5), kind=kLoop, calls=%fused_computation.17 | loop fusion | flops 2048 | bytes 12288 | tf_op jit(solution)/shard_map/convert_element_type | solution.py:170
  241.3 1.4 reshape.520
  (94 shorter events, 16.4 us)
Async XLA Ops:
  0.6 182.6 %copy-start = (bf16[1,256,2048]{2,1,0:T(8,128)(2,1)S(1)}, bf16[1,256,2048]{2,1,0:T(8,128)(2,1)}, u32[]{:S(2)}) copy-start(bf16[1,256,2048]{2,1,0:T(8,128)(2,1)} %param.38) | copy-start | bytes 3145732
  0.6 24.8 %copy-start.11 = (u32[32]{0:T(128)S(1)}, u32[32]{0:T(128)}, u32[]{:S(2)}) copy-start(u32[32]{0:T(128)} %constant.104) | copy-start | bytes 388
  0.7 32.3 %copy-start.4 = (bf16[128,512]{1,0:T(8,128)(2,1)S(1)}, bf16[128,512]{1,0:T(8,128)(2,1)}, u32[]{:S(2)}) copy-start(bf16[128,512]{1,0:T(8,128)(2,1)} %param.26) | copy-start | bytes 393220
  0.7 32.4 %copy-start.5 = (bf16[128,512]{1,0:T(8,128)(2,1)S(1)}, bf16[128,512]{1,0:T(8,128)(2,1)}, u32[]{:S(2)}) copy-start(bf16[128,512]{1,0:T(8,128)(2,1)} %param.25) | copy-start | bytes 393220
  0.7 32.6 %copy-start.6 = (bf16[128,256]{1,0:T(8,128)(2,1)S(1)}, bf16[128,256]{1,0:T(8,128)(2,1)}, u32[]{:S(2)}) copy-start(bf16[128,256]{1,0:T(8,128)(2,1)} %param.24) | copy-start | bytes 196612
  0.7 32.7 %copy-start.7 = (bf16[128,256]{1,0:T(8,128)(2,1)S(1)}, bf16[128,256]{1,0:T(8,128)(2,1)}, u32[]{:S(2)}) copy-start(bf16[128,256]{1,0:T(8,128)(2,1)} %param.23) | copy-start | bytes 196612
  4.1 21.9 %all-to-all-start.1 = ((bf16[1,16,128]{2,0,1:T(2,128)(2,1)}), bf16[1,16,128]{2,0,1:T(2,128)(2,1)S(1)}, u32[]{:S(2)}, u32[]{:S(2)}) async-start(bf16[1,16,128]{2,0,1:T(2,128)(2,1)} %convert_bitcast_fusion.3), calls=%async_computation.1 | async-start | bytes 16384 | tf_op jit(solution)/shard_map/all_to_all | solution.py:78
  13.5 102.5 %copy-start.10 = (f32[512]{0:T(512)S(1)}, f32[512]{0:T(512)}, u32[]{:S(2)}) copy-start(f32[512]{0:T(512)} %param.31) | copy-start | bytes 6148
  25.4 149.8 %copy-start.8 = (f32[2048]{0:T(1024)S(1)}, f32[2048]{0:T(1024)}, u32[]{:S(2)}) copy-start(f32[2048]{0:T(1024)} %param.33) | copy-start | bytes 24580
  25.4 149.8 %copy-start.2 = (bf16[2048,256]{1,0:T(8,128)(2,1)S(1)}, bf16[2048,256]{1,0:T(8,128)(2,1)}, u32[]{:S(2)}) copy-start(bf16[2048,256]{1,0:T(8,128)(2,1)} %param.39) | copy-start | bytes 3145732
  26.1 133.0 %all-to-all-start = ((bf16[1,16,128]{2,0,1:T(2,128)(2,1)}), bf16[1,16,128]{2,0,1:T(2,128)(2,1)S(1)}, u32[]{:S(2)}, u32[]{:S(2)}) async-start(bf16[1,16,128]{2,0,1:T(2,128)(2,1)} %bitcast), calls=%async_computation | async-start | bytes 16384 | tf_op jit(solution)/shard_map/all_to_all | solution.py:77
  33.5 142.0 %copy-start.3 = (bf16[2048,256]{1,0:T(8,128)(2,1)S(1)}, bf16[2048,256]{1,0:T(8,128)(2,1)}, u32[]{:S(2)}) copy-start(bf16[2048,256]{1,0:T(8,128)(2,1)} %param.40) | copy-start | bytes 3145732
  113.6 0.8 copy-start.1
  159.7 10.7 %all-to-all-start.4 = ((bf16[16,1,128]{2,1,0:T(2,128)(2,1)}), bf16[16,1,128]{2,1,0:T(2,128)(2,1)S(1)}, u32[]{:S(2)}, u32[]{:S(2)}) async-start(bf16[16,1,128]{2,1,0:T(2,128)(2,1)} %copy.73), calls=%async_computation.4 | async-start | bytes 16384 | tf_op jit(solution)/shard_map/all_to_all | solution.py:146
  170.4 11.0 %all-to-all-start.2 = ((bf16[16,12,128]{2,1,0:T(8,128)(2,1)}), bf16[16,12,128]{2,1,0:T(8,128)(2,1)S(1)}, u32[]{:S(2)}, u32[]{:S(2)}) async-start(bf16[16,12,128]{2,1,0:T(8,128)(2,1)} %reshape.471), calls=%async_computation.2 | async-start | bytes 131072 | tf_op jit(solution)/shard_map/all_to_all | solution.py:145
  175.8 18.9 %copy-start.9 = (f32[16,6]{0,1:T(8,128)S(1)}, f32[16,6]{0,1:T(8,128)}, u32[]{:S(2)}) copy-start(f32[16,6]{0,1:T(8,128)} %param.35) | copy-start | bytes 1156
  190.8 28.6 %all-to-all-start.5 = ((bf16[1,1,2048]{1,0,2:T(2,128)(2,1)}), bf16[1,1,2048]{1,0,2:T(2,128)(2,1)S(1)}, u32[]{:S(2)}, u32[]{:S(2)}) async-start(bf16[1,1,2048]{1,0,2:T(2,128)(2,1)} %copy.74), calls=%async_computation.5 | async-start | bytes 2097152 | tf_op jit(solution)/shard_map/all_to_all | solution.py:166
  219.3 22.0 %all-to-all-start.3 = ((bf16[16,2,768]{2,1,0:T(2,128)(2,1)}), bf16[16,2,768]{2,1,0:T(2,128)(2,1)S(1)}, u32[]{:S(2)}, u32[]{:S(2)}) async-start(bf16[16,2,768]{2,1,0:T(2,128)(2,1)} %reshape.519), calls=%async_computation.3 | async-start | bytes 98304 | tf_op jit(solution)/shard_map/all_to_all | solution.py:165
where the time goes:
time: 246 us; the launch traced here: 245 us
  blocking collectives  118 us (48%)
  other arithmetic  34.9 us (14%)
  starting transfers between devices  32.8 us (13%)
  local copies, waits for them, and re-layouts  19.3 us (8%)
  waiting for transfers between devices  18.4 us (7%)
  matrix products  18 us (7%)
  between operations  3.2 us (1%)
    unnamed x1, blocking collectives  78.2 us
    all_gather x1, blocking collectives, per_device(): shard_rows = lax.all_gather(mixed_heads, ('ep', 'tp'), axis=0, tiled=True)  36.5 us
    convert_element_type x1, other arithmetic, per_device(): back_shared.reshape(all_rows, -1).astype(jnp.float32)  15.2 us
    unnamed x1, other arithmetic  12.4 us
    all_to_all x1, waiting for transfers between devices, per_device(): lax.all_to_all(shared_out, 'ep', split_axis=2, concat_axis=0, tiled=True)  8.46 us
    all_to_all x1, starting transfers between devices, per_device(): lax.all_to_all(normed, 'ep', split_axis=1, concat_axis=0, tiled=True)  8.34 us
    all_to_all x1, starting transfers between devices, per_device(): lax.all_to_all(tokens, 'ep', split_axis=1, concat_axis=0, tiled=True)  6.91 us
    all_to_all x1, starting transfers between devices, per_device(): lax.all_to_all(routed_out, 'ep', split_axis=2, concat_axis=0, tiled=True)  6.75 us
  transfers between devices with their start and end apart: 6, of which 3 were waited for; matrix products, arithmetic and copies ran while one was open for 24% of the time, Pallas kernels for 0%

commit v1 on v0

v1 whole, which is shorter than its diff:
```python
import jax
import jax.numpy as jnp
from jax import lax
from jax.sharding import PartitionSpec as P

EPSILON = 1e-06
DECAY_TEMPER = 16.0
LANES = 128
F32 = jnp.float32
BF16 = jnp.bfloat16


def rms_scale(values):
    return lax.rsqrt(jnp.mean(values * values, axis=-1, keepdims=True) + EPSILON)


def exchange(blocks, axes):
    return lax.all_to_all(blocks, axes, split_axis=0, concat_axis=0, tiled=True)


def tp_sum(values):
    tp_size = lax.axis_size("tp")
    both = lax.all_gather(values, "tp", axis=0, tiled=False)
    total = both[0]
    for member in range(1, tp_size):
        total = total + both[member]
    return total


def per_device(
    tokens,
    norm_gain,
    w_query,
    w_key,
    w_value,
    w_outgate,
    decay_in,
    decay_out,
    decay_bias,
    gla_state,
    head_gain,
    w_output,
    moe_gain,
    expert_ids,
    route_weight,
    expert_gate,
    expert_up,
    expert_down,
    shared_gate,
    shared_up,
    shared_down,
):
    ep_size = lax.axis_size("ep")
    tp_size = lax.axis_size("tp")
    ep_index = lax.axis_index("ep")
    seq_dev, width = tokens.shape
    exp_dev = expert_gate.shape[0]
    all_rows = seq_dev * ep_size
    block = width // ep_size
    dk, dv = gla_state.shape[2:]
    heads_local = gla_state.shape[1]
    tok_float = tokens.astype(F32)
    normed = (tok_float * rms_scale(tok_float) * norm_gain).astype(BF16)
    outgoing = jnp.concatenate(
        [tokens.reshape(seq_dev, ep_size, block), normed.reshape(seq_dev, ep_size, block)], axis=0
    ).transpose(1, 0, 2)
    columns = exchange(outgoing, "ep")
    raw_columns = columns[:, :seq_dev].reshape(all_rows, block)
    normed_columns = columns[:, seq_dev:].reshape(all_rows, block)
    weights = (w_query, w_key, w_value, w_outgate)
    partial = jnp.concatenate(
        [jnp.dot(normed_columns, w, preferred_element_type=F32).astype(BF16) for w in weights],
        axis=1,
    )
    spans = partial.shape[1]
    partial = partial.reshape(ep_size, seq_dev * spans // LANES, LANES)
    joined = jnp.sum(exchange(partial, "ep").astype(F32), axis=0).reshape(seq_dev, spans)
    joined = joined.astype(BF16).astype(F32)
    edges = [0]
    for w in weights:
        edges.append(edges[-1] + w.shape[1])
    query, key, value, gate = (joined[:, edges[n] : edges[n + 1]] for n in range(4))
    decay_low = jnp.dot(normed, decay_in, preferred_element_type=F32).astype(BF16)
    decay_pre = jnp.dot(decay_low, decay_out, preferred_element_type=F32) + decay_bias
    decay_rate = jnp.exp(jax.nn.log_sigmoid(decay_pre) / DECAY_TEMPER)
    decay_rate = decay_rate.reshape(seq_dev, heads_local, dk)
    query = query.reshape(seq_dev, heads_local, dk) * dk ** (-0.5)
    key = key.reshape(seq_dev, heads_local, dk)
    value = value.reshape(seq_dev, heads_local, dv)
    gate = gate.reshape(seq_dev, heads_local, dv)
    new_state = decay_rate[..., None] * gla_state + key[..., None] * value[:, :, None, :]
    read_out = jnp.sum(query[..., None] * new_state, axis=2)
    mixed = (read_out * rms_scale(read_out) * head_gain * jax.nn.silu(gate)).astype(BF16)
    mixed = mixed.reshape(1, seq_dev * heads_local * dv // LANES, LANES)
    spread = exchange(
        jnp.broadcast_to(mixed, (ep_size * tp_size,) + mixed.shape[1:]), ("ep", "tp")
    )
    heads = spread.reshape(ep_size, tp_size, seq_dev, heads_local * dv)
    heads = heads.transpose(0, 2, 1, 3).reshape(all_rows, tp_size * heads_local * dv)
    attention = jnp.dot(heads, w_output, preferred_element_type=F32).astype(BF16)
    hidden = (raw_columns.astype(F32) + attention.astype(F32)).astype(BF16)
    rows = exchange(jnp.broadcast_to(hidden[None], (ep_size,) + hidden.shape), "ep")
    rows = rows.transpose(1, 0, 2).reshape(all_rows, width)
    row_float = rows.astype(F32)
    normal_rows = (row_float * rms_scale(row_float) * moe_gain).astype(BF16)
    routed = jnp.zeros((all_rows, width), F32)
    for number in range(exp_dev):
        expert = ep_index * exp_dev + number
        share = jnp.sum(jnp.where(expert_ids == expert, route_weight, 0.0), axis=1, keepdims=True)
        gate_values = jnp.dot(normal_rows, expert_gate[number], preferred_element_type=F32)
        upward = jnp.dot(normal_rows, expert_up[number], preferred_element_type=F32)
        active = (jax.nn.silu(gate_values) * upward).astype(BF16)
        routed = routed + share * jnp.dot(
            active, expert_down[number], preferred_element_type=F32
        )
    outgoing = routed.astype(BF16).reshape(all_rows, ep_size, block).transpose(1, 0, 2)
    back = exchange(outgoing, "ep")
    shared_values = jnp.dot(normal_rows, shared_gate, preferred_element_type=F32)
    shared_upward = jnp.dot(normal_rows, shared_up, preferred_element_type=F32)
    shared_active = (jax.nn.silu(shared_values) * shared_upward).astype(BF16)
    down_columns = lax.dynamic_slice_in_dim(shared_down, ep_index * block, block, 1)
    shared_part = jnp.dot(shared_active, down_columns, preferred_element_type=F32)
    moe_columns = tp_sum(shared_part + jnp.sum(back.astype(F32), axis=0))
    result = (hidden.astype(F32) + moe_columns).astype(BF16)
    return (result, new_state)


def solution(mesh):
    return jax.shard_map(
        per_device,
        mesh=mesh,
        in_specs=(
            P("ep", None),
            P(),
            P("ep", "tp"),
            P("ep", "tp"),
            P("ep", "tp"),
            P("ep", "tp"),
            P(),
            P(None, "tp"),
            P("tp"),
            P("ep", "tp", None, None),
            P(),
            P(None, "ep"),
            P(),
            P(),
            P(),
            P("ep", None, "tp"),
            P("ep", None, "tp"),
            P("ep", "tp", None),
            P(None, "tp"),
            P(None, "tp"),
            P("tp", None),
        ),
        out_specs=(P(None, "ep"), P("ep", "tp", None, None)),
        check_vma=False,
    )
```

time: 246 us -> 72 us (0.29)
  blocking collectives: 118 us -> 10.8 us
  other arithmetic: 34.9 us -> 4.46 us
  local copies, waits for them, and re-layouts: 19.3 us -> 2.13 us
  matrix products: 18 us -> 4.27 us
  starting transfers between devices: 32.8 us -> 19.1 us
  waiting for transfers between devices: 18.4 us -> 28.3 us
    unnamed x1 -> x0, blocking collectives: 78.2 us -> none
    all_gather x1, blocking collectives: 36.5 us -> 1.82 us  [tp_sum(): both = lax.all_gather(values, 'tp', axis=0, tiled=False)]
    convert_element_type x11 -> x1, other arithmetic: 16.1 us -> 0.6 us  [per_device(): result = (hidden.astype(F32) + moe_columns).astype(BF16)]
    dot_general x13 -> x10, matrix products: 18 us -> 4.27 us  [the longest x1 1.24 us: per_device(): jnp.dot(shared_active, down_columns, preferred_element_type=F32)]
    all_to_all x6 -> x4, starting transfers between devices: 32.8 us -> 19.1 us  [exchange(): return lax.all_to_all(blocks, axes, split_axis=0, concat_axis=0, tiled=True)]
    unnamed x1, other arithmetic: 12.4 us -> 0.01 us
    all_to_all x6 -> x4, waiting for transfers between devices: 18.4 us -> 28.3 us  [exchange(): return lax.all_to_all(blocks, axes, split_axis=0, concat_axis=0, tiled=True)]
    all_to_all x0 -> x1, blocking collectives: none -> 8.95 us  [exchange(): return lax.all_to_all(blocks, axes, split_axis=0, concat_axis=0, tiled=True)]
  transfers between devices with their start and end apart: 6 -> 4, of which waited for: 3 -> 4; matrix products, arithmetic and copies ran while one was open for 24% -> 2% of each run, Pallas kernels for 0% -> 0%
where the time goes in v1:
time: 72 us; the launch traced here: 71.4 us
  waiting for transfers between devices  28.3 us (39%)
  starting transfers between devices  19.1 us (27%)
  blocking collectives  10.8 us (15%)
  other arithmetic  4.46 us (6%)
  matrix products  4.27 us (6%)
  between operations  2.34 us (3%)
  local copies, waits for them, and re-layouts  2.13 us (3%)
    all_to_all x4, waiting for transfers between devices, exchange(): return lax.all_to_all(blocks, axes, split_axis=0, concat_axis=0, tiled=True)  28.3 us
    all_to_all x4, starting transfers between devices, exchange(): return lax.all_to_all(blocks, axes, split_axis=0, concat_axis=0, tiled=True)  19.1 us
    all_to_all x1, blocking collectives, exchange(): return lax.all_to_all(blocks, axes, split_axis=0, concat_axis=0, tiled=True)  8.95 us
    reduce_sum x3, other arithmetic, rms_scale(): jnp.mean(values * values, axis=-1, keepdims=True) + EPSILON  2.14 us
    all_gather x1, blocking collectives, tp_sum(): both = lax.all_gather(values, 'tp', axis=0, tiled=False)  1.82 us
  transfers between devices with their start and end apart: 4, of which 4 were waited for; matrix products, arithmetic and copies ran while one was open for 2% of the time, Pallas kernels for 0%

profile of v1, /device:TPU:0, one launch (start us, length us, event | category | flops | bytes accessed | tf_op | source)
XLA Modules:
  0.0 71.4 jit_solution(4791362143596041230)
XLA Ops:
  0.7 1.4 %multiply_reduce_fusion.1 = f32[]{:T(128)} fusion(bf16[1,2048]{1,0:T(2,128)(2,1)} %param.21), kind=kLoop, calls=%fused_computation.66 | loop fusion | flops 6143 | bytes 4100 | tf_op jit(solution)/shard_map/reduce_sum | solution.py:14
  2.8 0.6 maximum_bitcast_fusion
  3.5 8.5 %all-to-all-start = ((bf16[16,2,128]{2,1,0:T(2,128)(2,1)}), bf16[16,2,128]{2,1,0:T(2,128)(2,1)S(1)}, u32[]{:S(2)}, u32[]{:S(2)}) async-start(bf16[16,2,128]{2,1,0:T(2,128)(2,1)} %maximum_bitcast_fusion), calls=%async_computation | async-start | bytes 16384 | tf_op jit(solution)/shard_map/all_to_all | solution.py:18
  12.0 1.0 %fusion.16 = f32[1,256]{1,0:T(1,128)S(1)} fusion(bf16[16,256]{1,0:T(8,128)(2,1)} %param.28, bf16[2048,16]{0,1:T(8,128)(2,1)S(1)} %copy-done.18, f32[1,2048]{1,0:T(1,128)S(1)} %bitcast.113, bf16[1,2048]{1,0:T(2,128)(2,1)S(1)} %copy-done.10, f32[]{:T(128)S(6)} %rsqrt.16), kind=kOutput, calls=%fused_computation.24 | convolution fusion | flops 81936 | bytes 87044 | tf_op jit(solution)/shard_map/dot_general | solution.py:84
  13.0 6.2 %all-to-all-done = bf16[16,2,128]{2,1,0:T(2,128)(2,1)S(1)} async-done(((bf16[16,2,128]{2,1,0:T(2,128)(2,1)}), bf16[16,2,128]{2,1,0:T(2,128)(2,1)S(1)}, u32[]{:S(2)}, u32[]{:S(2)}) %all-to-all-start) | async-done | bytes 8224 | tf_op jit(solution)/shard_map/all_to_all | solution.py:18
  19.8 0.7 reshape.220
  20.4 3.6 %all-to-all-start.1 = ((bf16[16,12,128]{2,1,0:T(8,128)(2,1)}), bf16[16,12,128]{2,1,0:T(8,128)(2,1)S(1)}, u32[]{:S(2)}, u32[]{:S(2)}) async-start(bf16[16,12,128]{2,1,0:T(8,128)(2,1)} %reshape.220), calls=%async_computation.1 | async-start | bytes 131072 | tf_op jit(solution)/shard_map/all_to_all | solution.py:18
  24.1 7.5 %all-to-all-done.1 = bf16[16,12,128]{2,1,0:T(8,128)(2,1)S(1)} async-done(((bf16[16,12,128]{2,1,0:T(8,128)(2,1)}), bf16[16,12,128]{2,1,0:T(8,128)(2,1)S(1)}, u32[]{:S(2)}, u32[]{:S(2)}) %all-to-all-start.1) | async-done | bytes 49184 | tf_op jit(solution)/shard_map/all_to_all | solution.py:18
  31.7 1.0 %multiply_reduce_fusion = (f32[512]{0:T(512)S(1)}, f32[1,1,256,512]{3,2,1,0:T(8,128)}) fusion(f32[256]{0:T(256)S(1)} %bitcast.116, f32[512]{0:T(512)S(1)} %bitcast.111, f32[256]{0:T(256)S(1)} %bitcast.115, f32[1,1,256,512]{3,2,1,0:T(8,128)S(1)} %copy-done.5, f32[256]{0:T(256)S(1)} %fusion.52), kind=kLoop, calls=%fused_computation.25 | loop fusion | flops 654848 | bytes 1055744 | tf_op jit(solution)/shard_map/reduce_sum | solution.py:92
  32.7 0.6 multiply_reduce_fusion.2
  34.0 9.0 %all_to_all.25 = bf16[32,4,128]{2,1,0:T(4,128)(2,1)S(1)} all-to-all(bf16[32,4,128]{2,1,0:T(4,128)(2,1)S(1)} %broadcast_in_dim.13), channel_id=1, replica_groups=mesh['ep'=16,'tp'=2] {'ep','tp'}, dimensions={0} | all-to-all | bytes 65536 | tf_op jit(solution)/shard_map/all_to_all | solution.py:18
  43.0 0.2 fusion.8
  43.2 0.6 broadcast_in_dim.14
  43.8 3.5 %all-to-all-start.3 = ((bf16[16,16,128]{2,1,0:T(8,128)(2,1)}), bf16[16,16,128]{2,1,0:T(8,128)(2,1)S(1)}, u32[]{:S(2)}, u32[]{:S(2)}) async-start(bf16[16,16,128]{2,1,0:T(8,128)(2,1)} %broadcast_in_dim.14), calls=%async_computation.3 | async-start | bytes 131072 | tf_op jit(solution)/shard_map/all_to_all | solution.py:18
  47.4 7.5 %all-to-all-done.3 = bf16[16,16,128]{2,1,0:T(8,128)(2,1)S(1)} async-done(((bf16[16,16,128]{2,1,0:T(8,128)(2,1)}), bf16[16,16,128]{2,1,0:T(8,128)(2,1)S(1)}, u32[]{:S(2)}, u32[]{:S(2)}) %all-to-all-start.3) | async-done | bytes 65568 | tf_op jit(solution)/shard_map/all_to_all | solution.py:18
  55.0 0.3 fusion.14
  55.3 0.8 %fusion.1 = bf16[2,16,8,128]{3,2,1,0:T(8,128)(2,1)S(1)} fusion(bf16[1,256,2048]{2,1,0:T(8,128)(2,1)S(1)} %copy-done, bf16[1,2048,256]{2,1,0:T(8,128)(2,1)S(1)} %copy-done.2, f32[16]{0:T(128)S(1)} %select_reduce_fusion, f32[16,256]{1,0:T(8,128)S(1)} %fusion.14, bf16[16,16,128]{2,1,0:T(8,128)(2,1)S(1)} %all-to-all-done.3, f32[16,128]{1,0:T(8,128)S(1)} %bitcast.107, ...), kind=kOutput, calls=%fused_computation.2 | convolution fusion | flops 33775616 | bytes 2252928 | tf_op jit(solution)/shard_map/dot_general | solution.py:113
  56.1 0.7 copy.61
  56.7 3.5 %all-to-all-start.4 = ((bf16[16,16,128]{2,1,0:T(8,128)(2,1)}), bf16[16,16,128]{2,1,0:T(8,128)(2,1)S(1)}, u32[]{:S(2)}, u32[]{:S(2)}) async-start(bf16[16,16,128]{2,1,0:T(8,128)(2,1)} %bitcast.104), calls=%async_computation.4 | async-start | bytes 131072 | tf_op jit(solution)/shard_map/all_to_all | solution.py:18
  60.2 0.3 fusion.59
  60.5 7.2 %all-to-all-done.4 = bf16[16,16,128]{2,1,0:T(8,128)(2,1)S(1)} async-done(((bf16[16,16,128]{2,1,0:T(8,128)(2,1)}), bf16[16,16,128]{2,1,0:T(8,128)(2,1)S(1)}, u32[]{:S(2)}, u32[]{:S(2)}) %all-to-all-start.4) | async-done | bytes 65568 | tf_op jit(solution)/shard_map/all_to_all | solution.py:18
  67.7 1.2 %fusion.5 = f32[16,128]{1,0:T(8,128)S(1)} fusion(f32[16,128]{1,0:T(8,128)S(1)} %convert_reduce_fusion, bf16[2048,256]{1,0:T(8,128)(2,1)S(1)} %copy-done.4, bf16[256,2048]{1,0:T(8,128)(2,1)} %param.41, s32[]{:T(128)S(6)} %select_n.14, f32[16,256]{1,0:T(8,128)S(1)} %fusion.59, f32[2048]{0:T(1024)S(1)} %copy-done.7, f32[16]{0:T(128)S(1)} %add_rsqrt_fusion, ...), kind=kOutput, calls=%fused_computation.12 | convolution fusion | flops 17983488 | bytes 1220676 | tf_op jit(solution)/shard_map/dot_general | solution.py:122
  69.0 1.8 %all-gather = f32[32,128]{1,0:T(8,128)S(1)} all-gather(f32[16,128]{1,0:T(8,128)S(1)} %fusion.5), channel_id=2, replica_groups=mesh['ep'=16,'tp'=2] {'tp'}, dimensions={0}, use_global_device_ids=true | all-gather | bytes 24576 | tf_op jit(solution)/shard_map/all_gather | solution.py:23
  70.8 0.6 fusion.41
  (58 shorter events, 0.9 us)
Async XLA Ops:
  0.6 54.6 %copy-start = (bf16[1,256,2048]{2,1,0:T(8,128)(2,1)S(1)}, bf16[1,256,2048]{2,1,0:T(8,128)(2,1)}, u32[]{:S(2)}) copy-start(bf16[1,256,2048]{2,1,0:T(8,128)(2,1)} %param.38) | copy-start | bytes 3145732
  0.6 2.1 %copy-start.10 = (bf16[1,2048]{1,0:T(2,128)(2,1)S(1)}, bf16[1,2048]{1,0:T(2,128)(2,1)}, u32[]{:S(2)}) copy-start(bf16[1,2048]{1,0:T(2,128)(2,1)} %param.21) | copy-start | bytes 12292
  0.7 2.1 %copy-start.13 = (f32[2048]{0:T(1024)S(1)}, f32[2048]{0:T(1024)}, u32[]{:S(2)}) copy-start(f32[2048]{0:T(1024)} %param.22) | copy-start | bytes 24580
  0.7 11.3 %copy-start.18 = (bf16[2048,16]{0,1:T(8,128)(2,1)S(1)}, bf16[2048,16]{0,1:T(8,128)(2,1)}, u32[]{:S(2)}) copy-start(bf16[2048,16]{0,1:T(8,128)(2,1)} %param.27) | copy-start | bytes 196612
  0.7 18.5 %copy-start.8 = (bf16[128,512]{1,0:T(8,128)(2,1)S(1)}, bf16[128,512]{1,0:T(8,128)(2,1)}, u32[]{:S(2)}) copy-start(bf16[128,512]{1,0:T(8,128)(2,1)} %param.26) | copy-start | bytes 393220
  3.5 15.9 %copy-start.9 = (bf16[128,512]{1,0:T(8,128)(2,1)S(1)}, bf16[128,512]{1,0:T(8,128)(2,1)}, u32[]{:S(2)}) copy-start(bf16[128,512]{1,0:T(8,128)(2,1)} %param.25) | copy-start | bytes 393220
  3.5 16.0 %copy-start.11 = (bf16[128,256]{1,0:T(8,128)(2,1)S(1)}, bf16[128,256]{1,0:T(8,128)(2,1)}, u32[]{:S(2)}) copy-start(bf16[128,256]{1,0:T(8,128)(2,1)} %param.24) | copy-start | bytes 196612
  3.5 16.1 %copy-start.12 = (bf16[128,256]{1,0:T(8,128)(2,1)S(1)}, bf16[128,256]{1,0:T(8,128)(2,1)}, u32[]{:S(2)}) copy-start(bf16[128,256]{1,0:T(8,128)(2,1)} %param.23) | copy-start | bytes 196612
  3.5 15.7 %all-to-all-start = ((bf16[16,2,128]{2,1,0:T(2,128)(2,1)}), bf16[16,2,128]{2,1,0:T(2,128)(2,1)S(1)}, u32[]{:S(2)}, u32[]{:S(2)}) async-start(bf16[16,2,128]{2,1,0:T(2,128)(2,1)} %maximum_bitcast_fusion), calls=%async_computation | async-start | bytes 16384 | tf_op jit(solution)/shard_map/all_to_all | solution.py:18
  12.0 19.7 %copy-start.5 = (f32[1,1,256,512]{3,2,1,0:T(8,128)S(1)}, f32[1,1,256,512]{3,2,1,0:T(8,128)}, u32[]{:S(2)}) copy-start(f32[1,1,256,512]{3,2,1,0:T(8,128)} %param.30) | copy-start | bytes 1572868
  19.7 4.3 %copy-start.17 = (f32[256]{0:T(256)S(1)}, f32[256]{0:T(256)}, u32[]{:S(2)}) copy-start(f32[256]{0:T(256)} %param.29) | copy-start | bytes 3076
  20.4 34.5 %copy-start.1 = (bf16[1,2048,256]{2,1,0:T(8,128)(2,1)S(1)}, bf16[1,2048,256]{2,1,0:T(8,128)(2,1)}, u32[]{:S(2)}) copy-start(bf16[1,2048,256]{2,1,0:T(8,128)(2,1)} %param.36) | copy-start | bytes 3145732
  20.4 11.1 %all-to-all-start.1 = ((bf16[16,12,128]{2,1,0:T(8,128)(2,1)}), bf16[16,12,128]{2,1,0:T(8,128)(2,1)S(1)}, u32[]{:S(2)}, u32[]{:S(2)}) async-start(bf16[16,12,128]{2,1,0:T(8,128)(2,1)} %reshape.220), calls=%async_computation.1 | async-start | bytes 131072 | tf_op jit(solution)/shard_map/all_to_all | solution.py:18
  31.6 2.4 %copy-start.16 = (f32[512]{0:T(512)S(1)}, f32[512]{0:T(512)}, u32[]{:S(2)}) copy-start(f32[512]{0:T(512)} %param.31) | copy-start | bytes 6148
  31.7 11.3 %copy-start.6 = (bf16[1024,128]{1,0:T(8,128)(2,1)S(1)}, bf16[1024,128]{1,0:T(8,128)(2,1)}, u32[]{:S(2)}) copy-start(bf16[1024,128]{1,0:T(8,128)(2,1)} %param.32) | copy-start | bytes 786436
  31.7 15.6 %copy-start.14 = (f32[16,6]{0,1:T(8,128)S(1)}, f32[16,6]{0,1:T(8,128)}, u32[]{:S(2)}) copy-start(f32[16,6]{0,1:T(8,128)} %param.35) | copy-start | bytes 1156
  31.7 15.6 %copy-start.15 = (s32[16,6]{0,1:T(8,128)S(1)}, s32[16,6]{0,1:T(8,128)}, u32[]{:S(2)}) copy-start(s32[16,6]{0,1:T(8,128)} %param.34) | copy-start | bytes 1156
  31.7 23.2 %copy-start.7 = (f32[2048]{0:T(1024)S(1)}, f32[2048]{0:T(1024)}, u32[]{:S(2)}) copy-start(f32[2048]{0:T(1024)} %param.33) | copy-start | bytes 24580
  32.7 22.6 %copy-start.2 = (bf16[1,2048,256]{2,1,0:T(8,128)(2,1)S(1)}, bf16[1,2048,256]{2,1,0:T(8,128)(2,1)}, u32[]{:S(2)}) copy-start(bf16[1,2048,256]{2,1,0:T(8,128)(2,1)} %param.37) | copy-start | bytes 3145732
  43.8 11.0 %all-to-all-start.3 = ((bf16[16,16,128]{2,1,0:T(8,128)(2,1)}), bf16[16,16,128]{2,1,0:T(8,128)(2,1)S(1)}, u32[]{:S(2)}, u32[]{:S(2)}) async-start(bf16[16,16,128]{2,1,0:T(8,128)(2,1)} %broadcast_in_dim.14), calls=%async_computation.3 | async-start | bytes 131072 | tf_op jit(solution)/shard_map/all_to_all | solution.py:18
  55.3 4.9 %copy-start.3 = (bf16[2048,256]{1,0:T(8,128)(2,1)S(1)}, bf16[2048,256]{1,0:T(8,128)(2,1)}, u32[]{:S(2)}) copy-start(bf16[2048,256]{1,0:T(8,128)(2,1)} %param.39) | copy-start | bytes 3145732
  56.0 11.7 %copy-start.4 = (bf16[2048,256]{1,0:T(8,128)(2,1)S(1)}, bf16[2048,256]{1,0:T(8,128)(2,1)}, u32[]{:S(2)}) copy-start(bf16[2048,256]{1,0:T(8,128)(2,1)} %param.40) | copy-start | bytes 3145732
  56.7 11.0 %all-to-all-start.4 = ((bf16[16,16,128]{2,1,0:T(8,128)(2,1)}), bf16[16,16,128]{2,1,0:T(8,128)(2,1)S(1)}, u32[]{:S(2)}, u32[]{:S(2)}) async-start(bf16[16,16,128]{2,1,0:T(8,128)(2,1)} %bitcast.104), calls=%async_computation.4 | async-start | bytes 131072 | tf_op jit(solution)/shard_map/all_to_all | solution.py:18

commit v2 on v1

--- a/solution.py
+++ b/solution.py
@@ -59,23 +59,25 @@
     block = width // ep_size
     dk, dv = gla_state.shape[2:]
     heads_local = gla_state.shape[1]
+    everywhere = ("ep", "tp")
+    outgoing = tokens.reshape(seq_dev, ep_size, 1, block).transpose(1, 2, 0, 3)
+    outgoing = jnp.broadcast_to(outgoing, (ep_size, tp_size, seq_dev, block))
+    columns = exchange(outgoing.reshape(ep_size * tp_size, seq_dev, block), everywhere)
+    raw_columns = columns.reshape(ep_size, tp_size, seq_dev, block)[:, 0].reshape(all_rows, block)
+    gain_block = lax.dynamic_slice_in_dim(norm_gain, ep_index * block, block, 0)
+    gained_columns = (raw_columns.astype(F32) * gain_block).astype(BF16)
     tok_float = tokens.astype(F32)
-    normed = (tok_float * rms_scale(tok_float) * norm_gain).astype(BF16)
-    outgoing = jnp.concatenate(
-        [tokens.reshape(seq_dev, ep_size, block), normed.reshape(seq_dev, ep_size, block)], axis=0
-    ).transpose(1, 0, 2)
-    columns = exchange(outgoing, "ep")
-    raw_columns = columns[:, :seq_dev].reshape(all_rows, block)
-    normed_columns = columns[:, seq_dev:].reshape(all_rows, block)
+    tok_scale = rms_scale(tok_float)
+    normed = (tok_float * tok_scale * norm_gain).astype(BF16)
     weights = (w_query, w_key, w_value, w_outgate)
     partial = jnp.concatenate(
-        [jnp.dot(normed_columns, w, preferred_element_type=F32).astype(BF16) for w in weights],
+        [jnp.dot(gained_columns, w, preferred_element_type=F32).astype(BF16) for w in weights],
         axis=1,
     )
     spans = partial.shape[1]
     partial = partial.reshape(ep_size, seq_dev * spans // LANES, LANES)
     joined = jnp.sum(exchange(partial, "ep").astype(F32), axis=0).reshape(seq_dev, spans)
-    joined = joined.astype(BF16).astype(F32)
+    joined = (joined * tok_scale).astype(BF16).astype(F32)
     edges = [0]
     for w in weights:
         edges.append(edges[-1] + w.shape[1])
@@ -99,8 +101,13 @@
     heads = heads.transpose(0, 2, 1, 3).reshape(all_rows, tp_size * heads_local * dv)
     attention = jnp.dot(heads, w_output, preferred_element_type=F32).astype(BF16)
     hidden = (raw_columns.astype(F32) + attention.astype(F32)).astype(BF16)
-    rows = exchange(jnp.broadcast_to(hidden[None], (ep_size,) + hidden.shape), "ep")
-    rows = rows.transpose(1, 0, 2).reshape(all_rows, width)
+    part_rows = all_rows // tp_size
+    own_rows = lax.dynamic_slice_in_dim(hidden, lax.axis_index("tp") * part_rows, part_rows, 0)
+    rows = exchange(
+        jnp.broadcast_to(own_rows[None], (ep_size * tp_size,) + own_rows.shape), everywhere
+    )
+    rows = rows.reshape(ep_size, tp_size, part_rows, block).transpose(1, 2, 0, 3)
+    rows = rows.reshape(all_rows, width)
     row_float = rows.astype(F32)
     normal_rows = (row_float * rms_scale(row_float) * moe_gain).astype(BF16)
     routed = jnp.zeros((all_rows, width), F32)
@@ -113,14 +120,15 @@
         routed = routed + share * jnp.dot(
             active, expert_down[number], preferred_element_type=F32
         )
-    outgoing = routed.astype(BF16).reshape(all_rows, ep_size, block).transpose(1, 0, 2)
-    back = exchange(outgoing, "ep")
+    outgoing = routed.astype(BF16).reshape(all_rows, ep_size, 1, block).transpose(1, 2, 0, 3)
+    outgoing = jnp.broadcast_to(outgoing, (ep_size, tp_size, all_rows, block))
+    back = exchange(outgoing.reshape(ep_size * tp_size, all_rows, block), everywhere)
     shared_values = jnp.dot(normal_rows, shared_gate, preferred_element_type=F32)
     shared_upward = jnp.dot(normal_rows, shared_up, preferred_element_type=F32)
     shared_active = (jax.nn.silu(shared_values) * shared_upward).astype(BF16)
     down_columns = lax.dynamic_slice_in_dim(shared_down, ep_index * block, block, 1)
     shared_part = jnp.dot(shared_active, down_columns, preferred_element_type=F32)
-    moe_columns = tp_sum(shared_part + jnp.sum(back.astype(F32), axis=0))
+    moe_columns = tp_sum(shared_part) + jnp.sum(back.astype(F32), axis=0)
     result = (hidden.astype(F32) + moe_columns).astype(BF16)
     return (result, new_state)
 

time: 72 us -> 66.6 us (0.925)
  blocking collectives: 10.8 us -> 1.82 us
  waiting for transfers between devices: 28.3 us -> 31.6 us
  local copies, waits for them, and re-layouts: 2.13 us -> 4.33 us
  matrix products: 4.27 us -> 3.44 us
    all_to_all x1 -> x0, blocking collectives: 8.95 us -> none  [exchange(): return lax.all_to_all(blocks, axes, split_axis=0, concat_axis=0, tiled=True)]
    all_to_all x4 -> x5, waiting for transfers between devices: 28.3 us -> 31.6 us  [exchange(): return lax.all_to_all(blocks, axes, split_axis=0, concat_axis=0, tiled=True)]
    broadcast_in_dim x1 -> x5, local copies, waits for them, and re-layouts: 0.64 us -> 1.94 us  [the longest x2 0.68 us: per_device(): outgoing = jnp.broadcast_to(outgoing, (ep_size, tp_size, all_rows, block))]
    unnamed x1 -> x2, other arithmetic: 0.01 us -> 0.84 us
    reduce_sum x3, other arithmetic: 2.14 us -> 1.32 us  [rms_scale(): jnp.mean(values * values, axis=-1, keepdims=True) + EPSILON]
    dot_general x1, matrix products: 1 us -> 0.25 us  [per_device(): jnp.dot(decay_low, decay_out, preferred_element_type=F32) + decay_bias]
    all_to_all x4 -> x5, starting transfers between devices: 19.1 us -> 18.6 us  [exchange(): return lax.all_to_all(blocks, axes, split_axis=0, concat_axis=0, tiled=True)]
  transfers between devices with their start and end apart: 4 -> 5, of which waited for: 4 -> 5; matrix products, arithmetic and copies ran while one was open for 2% -> 4% of each run, Pallas kernels for 0% -> 0%
where the time goes in v2:
time: 66.6 us; the launch traced here: 66.2 us
  waiting for transfers between devices  31.6 us (47%)
  starting transfers between devices  18.6 us (28%)
  local copies, waits for them, and re-layouts  4.33 us (7%)
  other arithmetic  3.95 us (6%)
  matrix products  3.44 us (5%)
  between operations  2.4 us (4%)
  blocking collectives  1.82 us (3%)
    all_to_all x5, waiting for transfers between devices, exchange(): return lax.all_to_all(blocks, axes, split_axis=0, concat_axis=0, tiled=True)  31.6 us
    all_to_all x5, starting transfers between devices, exchange(): return lax.all_to_all(blocks, axes, split_axis=0, concat_axis=0, tiled=True)  18.6 us
    all_gather x1, blocking collectives, tp_sum(): both = lax.all_gather(values, 'tp', axis=0, tiled=False)  1.82 us
  transfers between devices with their start and end apart: 5, of which 5 were waited for; matrix products, arithmetic and copies ran while one was open for 4% of the time, Pallas kernels for 0%

profile of v2, /device:TPU:0, one launch (start us, length us, event | category | flops | bytes accessed | tf_op | source)
XLA Modules:
  0.0 66.2 jit_solution(4980736154856086967)
XLA Ops:
  0.7 0.8 %reduce.6 = bf16[2048]{0:T(1024)(128)(2,1)S(1)} reduce(bf16[1,2048]{1,0:T(2,128)(2,1)} %param.21, bf16[]{:T(256)} %constant.54), dimensions={0}, to_apply=%param.21.reduce_sub_computation | reduce | bytes 8194 | tf_op args[0]
  1.6 0.6 copy.39
  2.2 7.3 %all-to-all-start = ((bf16[32,1,128]{2,1,0:T(2,128)(2,1)}), bf16[32,1,128]{2,1,0:T(2,128)(2,1)S(1)}, u32[]{:S(2)}, u32[]{:S(2)}) async-start(bf16[32,1,128]{2,1,0:T(2,128)(2,1)} %copy.39), calls=%async_computation | async-start | bytes 32768 | tf_op jit(solution)/shard_map/all_to_all | solution.py:18
  9.5 0.6 multiply_reduce_fusion.1
  11.2 5.4 %all-to-all-done = bf16[32,1,128]{2,1,0:T(2,128)(2,1)S(1)} async-done(((bf16[32,1,128]{2,1,0:T(2,128)(2,1)}), bf16[32,1,128]{2,1,0:T(2,128)(2,1)S(1)}, u32[]{:S(2)}, u32[]{:S(2)}) %all-to-all-start) | async-done | bytes 8224 | tf_op jit(solution)/shard_map/all_to_all | solution.py:18
  17.2 0.7 %reshape.244 = bf16[16,12,128]{2,1,0:T(8,128)(2,1)} reshape(bf16[16,1536]{1,0:T(8,128)(2,1)S(1)} %pad_maximum_fusion) | data formatting | bytes 98304 | tf_op jit(solution)/shard_map/reshape | solution.py:78
  17.9 3.5 %all-to-all-start.1 = ((bf16[16,12,128]{2,1,0:T(8,128)(2,1)}), bf16[16,12,128]{2,1,0:T(8,128)(2,1)S(1)}, u32[]{:S(2)}, u32[]{:S(2)}) async-start(bf16[16,12,128]{2,1,0:T(8,128)(2,1)} %reshape.244), calls=%async_computation.1 | async-start | bytes 131072 | tf_op jit(solution)/shard_map/all_to_all | solution.py:18
  21.4 0.7 %copy-done.16 = f32[256]{0:T(256)S(1)} copy-done((f32[256]{0:T(256)S(1)}, f32[256]{0:T(256)}, u32[]{:S(2)}) %copy-start.16) | copy-done | bytes 1048
  22.1 6.8 %all-to-all-done.1 = bf16[16,12,128]{2,1,0:T(8,128)(2,1)S(1)} async-done(((bf16[16,12,128]{2,1,0:T(8,128)(2,1)}), bf16[16,12,128]{2,1,0:T(8,128)(2,1)S(1)}, u32[]{:S(2)}, u32[]{:S(2)}) %all-to-all-start.1) | async-done | bytes 49184 | tf_op jit(solution)/shard_map/all_to_all | solution.py:18
  29.0 1.0 %multiply_reduce_fusion = (f32[512]{0:T(512)S(1)}, f32[1,1,256,512]{3,2,1,0:T(8,128)}) fusion(f32[256]{0:T(256)S(1)} %bitcast.116, f32[512]{0:T(512)S(1)} %bitcast.113, f32[256]{0:T(256)S(1)} %bitcast.115, f32[1,1,256,512]{3,2,1,0:T(8,128)S(1)} %copy-done.5, f32[256]{0:T(256)S(1)} %fusion.65), kind=kLoop, calls=%fused_computation.24 | loop fusion | flops 654848 | bytes 1055744 | tf_op jit(solution)/shard_map/reduce_sum | solution.py:94
  30.0 0.6 multiply_reduce_fusion.2
  31.3 0.6 broadcast_in_dim.50
  31.9 2.5 %all-to-all-start.2 = ((bf16[32,4,128]{2,1,0:T(4,128)(2,1)}), bf16[32,4,128]{2,1,0:T(4,128)(2,1)S(1)}, u32[]{:S(2)}, u32[]{:S(2)}) async-start(bf16[32,4,128]{2,1,0:T(4,128)(2,1)} %broadcast_in_dim.50), calls=%async_computation.2 | async-start | bytes 65536 | tf_op jit(solution)/shard_map/all_to_all | solution.py:18
  34.5 7.3 %all-to-all-done.2 = bf16[32,4,128]{2,1,0:T(4,128)(2,1)S(1)} async-done(((bf16[32,4,128]{2,1,0:T(4,128)(2,1)}), bf16[32,4,128]{2,1,0:T(4,128)(2,1)S(1)}, u32[]{:S(2)}, u32[]{:S(2)}) %all-to-all-start.2) | async-done | bytes 32800 | tf_op jit(solution)/shard_map/all_to_all | solution.py:18
  41.9 0.6 broadcast_in_dim.51
  42.6 2.7 %all-to-all-start.3 = ((bf16[32,8,128]{2,1,0:T(8,128)(2,1)}), bf16[32,8,128]{2,1,0:T(8,128)(2,1)S(1)}, u32[]{:S(2)}, u32[]{:S(2)}) async-start(bf16[32,8,128]{2,1,0:T(8,128)(2,1)} %broadcast_in_dim.51), calls=%async_computation.3 | async-start | bytes 131072 | tf_op jit(solution)/shard_map/all_to_all | solution.py:18
  45.3 7.4 %all-to-all-done.3 = bf16[32,8,128]{2,1,0:T(8,128)(2,1)S(1)} async-done(((bf16[32,8,128]{2,1,0:T(8,128)(2,1)}), bf16[32,8,128]{2,1,0:T(8,128)(2,1)S(1)}, u32[]{:S(2)}, u32[]{:S(2)}) %all-to-all-start.3) | async-done | bytes 65568 | tf_op jit(solution)/shard_map/all_to_all | solution.py:18
  53.3 0.7 %fusion.1 = bf16[2,8,16,128]{3,1,2,0:T(8,128)(2,1)S(1)} fusion(bf16[1,256,2048]{2,1,0:T(8,128)(2,1)S(1)} %copy-done, bf16[1,2048,256]{2,1,0:T(8,128)(2,1)S(1)} %copy-done.1, f32[16]{0:T(128)S(1)} %select_reduce_fusion, bf16[2,8,16,128]{3,2,1,0:T(8,128)(2,1)S(1)} %copy.68, f32[16,256]{1,0:T(8,128)S(1)} %fusion.13), kind=kOutput, calls=%fused_computation.2 | convolution fusion | flops 33644544 | bytes 2244672 | tf_op jit(solution)/shard_map/dot_general | solution.py:120
  54.1 0.7 %broadcast_in_dim.54 = bf16[16,2,16,128]{3,2,1,0:T(8,128)(2,1)} broadcast(bf16[16,16,128]{2,1,0:T(8,128)(2,1)S(1)} %copy.43), dimensions={0,2,3} | broadcast | bytes 196608 | tf_op jit(solution)/shard_map/broadcast_in_dim | solution.py:124
  54.8 2.6 %all-to-all-start.4 = ((bf16[32,16,128]{2,1,0:T(8,128)(2,1)}), bf16[32,16,128]{2,1,0:T(8,128)(2,1)S(1)}, u32[]{:S(2)}, u32[]{:S(2)}) async-start(bf16[32,16,128]{2,1,0:T(8,128)(2,1)} %bitcast.22), calls=%async_computation.4 | async-start | bytes 262144 | tf_op jit(solution)/shard_map/all_to_all | solution.py:18
  57.6 1.2 %fusion.4 = f32[16,128]{1,0:T(8,128)S(1)} fusion(bf16[2048,256]{1,0:T(8,128)(2,1)S(1)} %copy-done.4, bf16[256,2048]{1,0:T(8,128)(2,1)} %param.41, s32[]{:T(128)S(6)} %select_n.17, f32[16,256]{1,0:T(8,128)S(1)} %fusion.72, f32[2,8,16,128]{3,2,1,0:T(8,128)S(1)} %copy.67, f32[2048]{0:T(1024)S(1)} %copy-done.9, f32[16]{0:T(128)S(1)} %rsqrt.23), kind=kOutput, calls=%fused_computation.11 | convolution fusion | flops 17948672 | bytes 1278020 | tf_op jit(solution)/shard_map/dot_general | solution.py:130
  58.9 1.8 %all-gather = f32[32,128]{1,0:T(8,128)S(1)} all-gather(f32[16,128]{1,0:T(8,128)S(1)} %fusion.4), channel_id=2, replica_groups=mesh['ep'=16,'tp'=2] {'tp'}, dimensions={0}, use_global_device_ids=true | all-gather | bytes 24576 | tf_op jit(solution)/shard_map/all_gather | solution.py:23
  60.7 4.8 %all-to-all-done.4 = bf16[32,16,128]{2,1,0:T(8,128)(2,1)S(1)} async-done(((bf16[32,16,128]{2,1,0:T(8,128)(2,1)}), bf16[32,16,128]{2,1,0:T(8,128)(2,1)S(1)}, u32[]{:S(2)}, u32[]{:S(2)}) %all-to-all-start.4) | async-done | bytes 131104 | tf_op jit(solution)/shard_map/all_to_all | solution.py:18
  65.6 0.6 fusion.42
  (72 shorter events, 2.2 us)
Async XLA Ops:
  0.6 52.7 %copy-start = (bf16[1,256,2048]{2,1,0:T(8,128)(2,1)S(1)}, bf16[1,256,2048]{2,1,0:T(8,128)(2,1)}, u32[]{:S(2)}) copy-start(bf16[1,256,2048]{2,1,0:T(8,128)(2,1)} %param.38) | copy-start | bytes 3145732
  0.6 10.2 %copy-start.17 = (bf16[2048,16]{0,1:T(8,128)(2,1)S(1)}, bf16[2048,16]{0,1:T(8,128)(2,1)}, u32[]{:S(2)}) copy-start(bf16[2048,16]{0,1:T(8,128)(2,1)} %param.27) | copy-start | bytes 196612
  1.5 8.0 %copy-start.12 = (bf16[1,2048]{1,0:T(2,128)(2,1)S(1)}, bf16[1,2048]{1,0:T(2,128)(2,1)}, u32[]{:S(2)}) copy-start(bf16[1,2048]{1,0:T(2,128)(2,1)} %param.21) | copy-start | bytes 12292
  1.5 9.3 %copy-start.18 = (bf16[16,256]{1,0:T(8,128)(2,1)S(1)}, bf16[16,256]{1,0:T(8,128)(2,1)}, u32[]{:S(2)}) copy-start(bf16[16,256]{1,0:T(8,128)(2,1)} %param.28) | copy-start | bytes 24580
  1.5 9.3 %copy-start.19 = (f32[2048]{0:T(1024)S(1)}, f32[2048]{0:T(1024)}, u32[]{:S(2)}) copy-start(f32[2048]{0:T(1024)} %param.22) | copy-start | bytes 24580
  1.5 15.1 %copy-start.7 = (bf16[128,512]{1,0:T(8,128)(2,1)S(1)}, bf16[128,512]{1,0:T(8,128)(2,1)}, u32[]{:S(2)}) copy-start(bf16[128,512]{1,0:T(8,128)(2,1)} %param.25) | copy-start | bytes 393220
  2.2 14.4 %all-to-all-start = ((bf16[32,1,128]{2,1,0:T(2,128)(2,1)}), bf16[32,1,128]{2,1,0:T(2,128)(2,1)S(1)}, u32[]{:S(2)}, u32[]{:S(2)}) async-start(bf16[32,1,128]{2,1,0:T(2,128)(2,1)} %copy.39), calls=%async_computation | async-start | bytes 32768 | tf_op jit(solution)/shard_map/all_to_all | solution.py:18
  10.9 5.9 %copy-start.8 = (bf16[128,512]{1,0:T(8,128)(2,1)S(1)}, bf16[128,512]{1,0:T(8,128)(2,1)}, u32[]{:S(2)}) copy-start(bf16[128,512]{1,0:T(8,128)(2,1)} %param.26) | copy-start | bytes 393220
  10.9 6.0 %copy-start.10 = (bf16[128,256]{1,0:T(8,128)(2,1)S(1)}, bf16[128,256]{1,0:T(8,128)(2,1)}, u32[]{:S(2)}) copy-start(bf16[128,256]{1,0:T(8,128)(2,1)} %param.24) | copy-start | bytes 196612
  10.9 6.1 %copy-start.11 = (bf16[128,256]{1,0:T(8,128)(2,1)S(1)}, bf16[128,256]{1,0:T(8,128)(2,1)}, u32[]{:S(2)}) copy-start(bf16[128,256]{1,0:T(8,128)(2,1)} %param.23) | copy-start | bytes 196612
  11.1 17.8 %copy-start.5 = (f32[1,1,256,512]{3,2,1,0:T(8,128)S(1)}, f32[1,1,256,512]{3,2,1,0:T(8,128)}, u32[]{:S(2)}) copy-start(f32[1,1,256,512]{3,2,1,0:T(8,128)} %param.30) | copy-start | bytes 1572868
  17.9 11.0 %all-to-all-start.1 = ((bf16[16,12,128]{2,1,0:T(8,128)(2,1)}), bf16[16,12,128]{2,1,0:T(8,128)(2,1)S(1)}, u32[]{:S(2)}, u32[]{:S(2)}) async-start(bf16[16,12,128]{2,1,0:T(8,128)(2,1)} %reshape.244), calls=%async_computation.1 | async-start | bytes 131072 | tf_op jit(solution)/shard_map/all_to_all | solution.py:18
  28.9 12.8 %copy-start.6 = (bf16[1024,128]{1,0:T(8,128)(2,1)S(1)}, bf16[1024,128]{1,0:T(8,128)(2,1)}, u32[]{:S(2)}) copy-start(bf16[1024,128]{1,0:T(8,128)(2,1)} %param.32) | copy-start | bytes 786436
  28.9 2.3 %copy-start.15 = (f32[512]{0:T(512)S(1)}, f32[512]{0:T(512)}, u32[]{:S(2)}) copy-start(f32[512]{0:T(512)} %param.31) | copy-start | bytes 6148
  29.0 24.1 %copy-start.2 = (bf16[1,2048,256]{2,1,0:T(8,128)(2,1)S(1)}, bf16[1,2048,256]{2,1,0:T(8,128)(2,1)}, u32[]{:S(2)}) copy-start(bf16[1,2048,256]{2,1,0:T(8,128)(2,1)} %param.36) | copy-start | bytes 3145732
  31.9 9.8 %all-to-all-start.2 = ((bf16[32,4,128]{2,1,0:T(4,128)(2,1)}), bf16[32,4,128]{2,1,0:T(4,128)(2,1)S(1)}, u32[]{:S(2)}, u32[]{:S(2)}) async-start(bf16[32,4,128]{2,1,0:T(4,128)(2,1)} %broadcast_in_dim.50), calls=%async_computation.2 | async-start | bytes 65536 | tf_op jit(solution)/shard_map/all_to_all | solution.py:18
  41.9 3.3 %copy-start.13 = (f32[16,6]{0,1:T(8,128)S(1)}, f32[16,6]{0,1:T(8,128)}, u32[]{:S(2)}) copy-start(f32[16,6]{0,1:T(8,128)} %param.35) | copy-start | bytes 1156
  41.9 3.3 %copy-start.14 = (s32[16,6]{0,1:T(8,128)S(1)}, s32[16,6]{0,1:T(8,128)}, u32[]{:S(2)}) copy-start(s32[16,6]{0,1:T(8,128)} %param.34) | copy-start | bytes 1156
  41.9 11.0 %copy-start.9 = (f32[2048]{0:T(1024)S(1)}, f32[2048]{0:T(1024)}, u32[]{:S(2)}) copy-start(f32[2048]{0:T(1024)} %param.33) | copy-start | bytes 24580
  42.6 10.7 %copy-start.1 = (bf16[1,2048,256]{2,1,0:T(8,128)(2,1)S(1)}, bf16[1,2048,256]{2,1,0:T(8,128)(2,1)}, u32[]{:S(2)}) copy-start(bf16[1,2048,256]{2,1,0:T(8,128)(2,1)} %param.37) | copy-start | bytes 3145732
  42.6 10.1 %all-to-all-start.3 = ((bf16[32,8,128]{2,1,0:T(8,128)(2,1)}), bf16[32,8,128]{2,1,0:T(8,128)(2,1)S(1)}, u32[]{:S(2)}, u32[]{:S(2)}) async-start(bf16[32,8,128]{2,1,0:T(8,128)(2,1)} %broadcast_in_dim.51), calls=%async_computation.3 | async-start | bytes 131072 | tf_op jit(solution)/shard_map/all_to_all | solution.py:18
  53.3 4.0 %copy-start.3 = (bf16[2048,256]{1,0:T(8,128)(2,1)S(1)}, bf16[2048,256]{1,0:T(8,128)(2,1)}, u32[]{:S(2)}) copy-start(bf16[2048,256]{1,0:T(8,128)(2,1)} %param.39) | copy-start | bytes 3145732
  54.1 3.6 %copy-start.4 = (bf16[2048,256]{1,0:T(8,128)(2,1)S(1)}, bf16[2048,256]{1,0:T(8,128)(2,1)}, u32[]{:S(2)}) copy-start(bf16[2048,256]{1,0:T(8,128)(2,1)} %param.40) | copy-start | bytes 3145732
  54.8 10.8 %all-to-all-start.4 = ((bf16[32,16,128]{2,1,0:T(8,128)(2,1)}), bf16[32,16,128]{2,1,0:T(8,128)(2,1)S(1)}, u32[]{:S(2)}, u32[]{:S(2)}) async-start(bf16[32,16,128]{2,1,0:T(8,128)(2,1)} %bitcast.22), calls=%async_computation.4 | async-start | bytes 262144 | tf_op jit(solution)/shard_map/all_to_all | solution.py:18
  (1 other events, 0.7 us)
